TPU v7x, 128 devices: a whole 4x4x4 slice. The times are simulated.
128 devices in a mesh: ep: 128 (over z, y, x, core).
Axes of the slice: x: 4, y: 4, z: 4, core: 2. Of those that a mesh axis runs over, the one named last changes fastest.
Arguments:
- tokens: bfloat16 [512, 2048], P('ep'), may hold values from -6 to 6
- norm_gain: float32 [2048], replicated, may hold values from 0.1 to 1.9
- routes: int32 [512, 2], P('ep'), may hold values from 0 to 7, all different within a row; in each aligned block of 4 rows (0 to 3, 4 to 7, ...) at most 2 rows name the same one
- route_weight: float32 [512, 2], P('ep'), may hold values from 0.1 to 1
- gate_weight: bfloat16 [2048, 57344], P(None, 'ep'), may hold values from -0.125 to 0.125
- up_weight: bfloat16 [2048, 57344], P(None, 'ep'), may hold values from -0.125 to 0.125
- down_weight: bfloat16 [57344, 2048], P('ep'), may hold values from -0.0625 to 0.0625
Outputs:
- mixed: bfloat16 [512, 2048], P('ep')
Inputs may be any that keep to these rules, and one draw needn't show every extreme that they name: `routes`: each row names two different experts of 0 to 7; among the rows of one device no expert is named by more than 2 rows, and in some device one expert is named by exactly 2.
All inputs are finite; a program needn't handle non-finite values.
Results may differ from a plain program's by a relative error of at most 0.0095.
Values may be sent and summed in bfloat16 or wider, within the bound.
A program may use at most 64 MiB of HBM per device.

v0:
```python
import jax
import jax.numpy as jnp
from jax import lax
from jax.sharding import PartitionSpec as P

GROUP = 16


epsilon = 1e-06


def expert_rows(rows, gate_part, up_part, down_part):
    gate = jnp.dot(rows, gate_part, preferred_element_type=jnp.float32)
    upper = jnp.dot(rows, up_part, preferred_element_type=jnp.float32)
    hidden = (jax.nn.silu(gate) * upper).astype(jnp.bfloat16)
    return jnp.dot(hidden, down_part, preferred_element_type=jnp.float32)


def normalize(tokens, norm_gain):
    values = tokens.astype(jnp.float32)
    scale = lax.rsqrt(jnp.mean(values * values, axis=-1, keepdims=True) + epsilon)
    return (values * scale * norm_gain).astype(jnp.bfloat16)


def on_device(tokens, norm_gain, routes, route_weight, gate_weight, up_weight, down_weight):
    normed = normalize(tokens, norm_gain)
    tok_count = tokens.shape[0]
    width = tokens.shape[1]
    devices = lax.axis_size("ep")
    experts = devices // GROUP
    most = min(tok_count, max(tok_count // 2, (2 * tok_count + experts - 1) // experts))
    expert_ids = lax.broadcasted_iota(jnp.int32, (1, experts), 1)
    pairs = 2 * tok_count
    flat_experts = routes.reshape(pairs)
    flat_weights = route_weight.reshape(pairs)
    onehot = (flat_experts[:, None] == expert_ids).astype(jnp.int32)
    earlier = jnp.cumsum(onehot, axis=0) - onehot
    slot = jnp.sum(earlier * onehot, axis=1)
    target = flat_experts * most + slot
    slot_ids = lax.broadcasted_iota(jnp.int32, (experts * most, pairs), 0)
    placed = (slot_ids == target[None, :]).astype(jnp.float32)
    pair_rows = lax.broadcasted_iota(jnp.int32, (pairs, tok_count), 0) // 2
    pair_cols = lax.broadcasted_iota(jnp.int32, (pairs, tok_count), 1)
    pair_token = (pair_rows == pair_cols).astype(jnp.float32)
    picker = jnp.dot(placed, pair_token, precision=lax.Precision.HIGHEST)
    outgoing = jnp.dot(
        picker.astype(jnp.bfloat16), normed, preferred_element_type=jnp.float32
    ).astype(jnp.bfloat16)
    outgoing = jnp.broadcast_to(
        outgoing.reshape(experts, 1, most, width), (experts, GROUP, most, width)
    )
    outgoing = outgoing.reshape(devices, most, width)
    received = lax.all_to_all(outgoing, "ep", split_axis=0, concat_axis=0, tiled=True)
    count = received.shape[1]
    flat = received.reshape(devices * count, width)
    result = expert_rows(flat, gate_weight, up_weight, down_weight).reshape(devices, count, width)
    back = lax.all_to_all(
        result.astype(jnp.bfloat16), "ep", split_axis=0, concat_axis=0, tiled=True
    ).astype(result.dtype)
    summed = jnp.sum(back.reshape(experts, GROUP, most, width), axis=1).reshape(
        experts * most, width
    )
    weighted_pairs = pair_token.T * flat_weights[None, :]
    selector = jnp.dot(weighted_pairs, placed.T, precision=lax.Precision.HIGHEST)
    mixed = jnp.dot(selector, summed, precision=lax.Precision.HIGHEST)
    return mixed.astype(jnp.bfloat16)


def solution(mesh):
    return jax.shard_map(
        on_device,
        mesh=mesh,
        in_specs=(
            P("ep", None),
            P(),
            P("ep", None),
            P("ep", None),
            P(None, "ep"),
            P(None, "ep"),
            P("ep", None),
        ),
        out_specs=P("ep", None),
        check_vma=False,
    )
```

profile of v0, /device:TPU:1, one launch (start us, length us, event | category | flops | bytes accessed | tf_op | source)
XLA Modules:
  0.0 71.2 jit_solution(5208679083883799464)
XLA Ops:
  0.0 0.0 copy-start
  0.0 1.0 %fusion.7 = f32[4]{0:T(128)S(1)} fusion(bf16[4,2048]{1,0:T(4,128)(2,1)} %param.7), kind=kLoop, calls=%fused_computation.15 | loop fusion | flops 24572 | bytes 16400 | tf_op jit(solution)/shard_map/reduce_sum | solution.py:21
  1.0 0.8 %copy.13 = s32[4,2]{1,0:T(4,128)S(1)} copy(s32[4,2]{0,1:T(2,128)} %param.9) | data formatting | bytes 64 | tf_op args[2]
  1.8 0.1 reshape.41
  1.9 0.1 fusion.16
  2.0 0.2 select_reduce_fusion
  2.2 0.3 convolution_convert_fusion.3
  2.4 0.9 %convolution_convert_fusion.1 = bf16[16,2048]{1,0:T(8,128)(2,1)S(1)} fusion(bf16[16,4]{0,1:T(4,128)(2,1)S(1)} %convolution_convert_fusion.3, bf16[4,2048]{1,0:T(4,128)(2,1)} %param.7, f32[2048]{0:T(1024)} %param.8, f32[4]{0:T(128)S(1)} %add_rsqrt_fusion), kind=kOutput, calls=%fused_computation.1 | convolution fusion | flops 327680 | bytes 90256 | tf_op jit(solution)/shard_map/dot_general | solution.py:46
  3.4 0.1 broadcast_in_dim.4
  3.4 0.6 broadcast_in_dim.5
  4.1 30.6 %all_to_all.10 = bf16[128,2,2048]{2,1,0:T(2,128)(2,1)} all-to-all(bf16[128,2,2048]{2,1,0:T(2,128)(2,1)S(1)} %bitcast.12), channel_id=1, replica_groups=mesh['ep'=128] {'ep'}, dimensions={0} | all-to-all | bytes 2097152 | tf_op jit(solution)/shard_map/all_to_all | solution.py:53
  34.7 1.5 %reshape.43 = bf16[256,2048]{1,0:T(8,128)(2,1)S(1)} reshape(bf16[128,2,2048]{2,1,0:T(2,128)(2,1)} %all_to_all.10) | data formatting | bytes 2097152 | tf_op jit(solution)/shard_map/reshape | solution.py:55
  36.2 2.2 %fusion.28 = f32[256,448]{0,1:T(8,128)S(1)} fusion(bf16[256,2048]{1,0:T(8,128)(2,1)S(1)} %reshape.43, bf16[2048,448]{0,1:T(8,128)(2,1)} %param.11), kind=kOutput, calls=%fused_computation.47 | convolution fusion | flops 469762048 | bytes 3342336 | tf_op jit(solution)/shard_map/dot_general | solution.py:13
  38.3 0.0 copy-done
  38.3 4.8 %convolution_convert_fusion = bf16[256,2048]{1,0:T(8,128)(2,1)} fusion(bf16[448,2048]{1,0:T(8,128)(2,1)S(1)} %copy-done, bf16[256,2048]{1,0:T(8,128)(2,1)S(1)} %reshape.43, bf16[2048,448]{0,1:T(8,128)(2,1)} %param.12, f32[256,448]{0,1:T(8,128)S(1)} %fusion.28), kind=kOutput, calls=%fused_computation | convolution fusion | flops 940736512 | bytes 6225920 | tf_op jit(solution)/shard_map/dot_general | solution.py:16
  43.1 0.0 copy-start.1
  43.1 2.6 %convert_element_type.38 = bf16[128,2,2048]{2,1,0:T(2,128)(2,1)} reshape(bf16[256,2048]{1,0:T(8,128)(2,1)} %convolution_convert_fusion) | data formatting | bytes 2097152 | tf_op jit(solution)/shard_map/convert_element_type | solution.py:58
  45.7 4.4 %all-to-all-start.1 = ((bf16[128,2,2048]{2,1,0:T(2,128)(2,1)}), bf16[128,2,2048]{2,1,0:T(2,128)(2,1)S(1)}, u32[]{:S(2)}, u32[]{:S(2)}) async-start(bf16[128,2,2048]{2,1,0:T(2,128)(2,1)} %convert_element_type.38), calls=%async_computation.1 | async-start | bytes 2097152 | tf_op jit(solution)/shard_map/all_to_all | solution.py:57
  50.1 0.0 copy-done.1
  50.1 0.1 copy.12
  50.2 0.1 mul.46
  50.3 0.1 fusion.13
  50.4 19.0 %all-to-all-done.1 = bf16[128,2,2048]{2,1,0:T(2,128)(2,1)S(1)} async-done(((bf16[128,2,2048]{2,1,0:T(2,128)(2,1)}), bf16[128,2,2048]{2,1,0:T(2,128)(2,1)S(1)}, u32[]{:S(2)}, u32[]{:S(2)}) %all-to-all-start.1) | async-done | bytes 1048608 | tf_op jit(solution)/shard_map/all_to_all | solution.py:57
  69.4 0.8 %convert_reduce_fusion = f32[8,2,2048]{2,1,0:T(2,128)S(1)} fusion(bf16[128,2,2048]{2,1,0:T(2,128)(2,1)S(1)} %all-to-all-done.1), kind=kLoop, calls=%fused_computation.3 | loop fusion | flops 1015808 | bytes 1179648 | tf_op jit(solution)/shard_map/reduce_sum | solution.py:60
  70.3 0.1 reshape.46
  70.4 0.8 %convolution_convert_fusion.2 = bf16[4,2048]{1,0:T(4,128)(2,1)} fusion(f32[4,16]{1,0:T(4,128)S(1)} %fusion.13, f32[16,2048]{1,0:T(8,128)S(1)} %reshape.46), kind=kOutput, calls=%fused_computation.2 | convolution fusion | flops 1581056 | bytes 147712 | tf_op jit(solution)/shard_map/dot_general | solution.py:65
  (5 shorter events, 0.1 us)
Async XLA Ops:
  0.0 38.3 %copy-start = (bf16[448,2048]{1,0:T(8,128)(2,1)S(1)}, bf16[448,2048]{1,0:T(8,128)(2,1)}, u32[]{:S(2)}) copy-start(bf16[448,2048]{1,0:T(8,128)(2,1)} %param.13) | copy-start | bytes 5505028
  43.1 7.0 %copy-start.1 = (f32[4,2]{0,1:T(2,128)S(1)}, f32[4,2]{0,1:T(2,128)}, u32[]{:S(2)}) copy-start(f32[4,2]{0,1:T(2,128)} %param.10) | copy-start | bytes 100
  45.7 23.8 %all-to-all-start.1 = ((bf16[128,2,2048]{2,1,0:T(2,128)(2,1)}), bf16[128,2,2048]{2,1,0:T(2,128)(2,1)S(1)}, u32[]{:S(2)}, u32[]{:S(2)}) async-start(bf16[128,2,2048]{2,1,0:T(2,128)(2,1)} %convert_element_type.38), calls=%async_computation.1 | async-start | bytes 2097152 | tf_op jit(solution)/shard_map/all_to_all | solution.py:57
where the time goes:
time: 71.6 us; the launch traced here: 71.2 us
  blocking collectives  30.6 us (43%)
  waiting for transfers between devices  19 us (27%)
  matrix products  9.07 us (13%)
  local copies, waits for them, and re-layouts  5.84 us (8%)
  starting transfers between devices  4.42 us (6%)
  other arithmetic  2.13 us (3%)
    all_to_all x1, blocking collectives, on_device(): lax.all_to_all(outgoing, 'ep', split_axis=0, concat_axis=0, tiled=True)  30.6 us
    all_to_all x1, waiting for transfers between devices, on_device(): lax.all_to_all(result.astype(jnp.bfloat16), 'ep', split_axis=0, concat_ax...  19 us
    dot_general x1, matrix products, expert_rows(): return jnp.dot(hidden, down_part, preferred_element_type=jnp.float32)  4.77 us
    all_to_all x1, starting transfers between devices, on_device(): lax.all_to_all(result.astype(jnp.bfloat16), 'ep', split_axis=0, concat_ax...  4.42 us
    convert_element_type x1, local copies, waits for them, and re-layouts, on_device(): result.astype(jnp.bfloat16)  2.56 us
    dot_general x1, matrix products, expert_rows(): gate = jnp.dot(rows, gate_part, preferred_element_type=jnp.float32)  2.17 us
    reshape x1, local copies, waits for them, and re-layouts, on_device(): flat = received.reshape(devices * count, width)  1.46 us
  transfers between devices with their start and end apart: 1, of which 1 were waited for; matrix products, arithmetic and copies ran while one was open for 0% of the time, Pallas kernels for 0%

commit v1 on v0

v1 whole, which is shorter than its diff:
```python
import functools

import jax
import jax.numpy as jnp
from jax import lax
from jax.experimental import pallas as pl
from jax.experimental.pallas import tpu as pltpu
from jax.sharding import PartitionSpec as P

MESH = pl.DeviceIdType.MESH
GROUP = 16
SIDE = 4
CHIPS = SIDE**3
EPSILON = 1e-06
BATCHES = 2
PER = CHIPS // BATCHES
PARTS = SIDE // BATCHES


def offset_of(batch, i):
    dz, dy = (i // SIDE) % SIDE, i % SIDE
    part = batch * PARTS + i // (SIDE * SIDE)
    return dz, dy, (part + 2 * SIDE - dz - dy) % SIDE


def kernel(
    tokens_hbm, gain_hbm, routes_hbm, mix_hbm, gate_hbm, up_hbm, down_hbm, out_ref,
    tokens, gain, routes, mix, gate, up, down, outgoing, rows, part_out, part_in, own, summed, back,
    load_sem, small_sem, disp_send, disp_recv, fwd_send, fwd_recv, red_send, red_recv, back_send, back_recv,
):
    width = tokens.shape[1]
    count = tokens.shape[0]
    me = lax.axis_index("ep")
    core = me % 2
    chip = me // 2
    x, y, z = chip % SIDE, (chip // SIDE) % SIDE, chip // (SIDE * SIDE)
    partner = me + 1 - 2 * core

    def ahead(off):
        dz, dy, dx = off
        return ((((z + dz) % SIDE) * SIDE + (y + dy) % SIDE) * SIDE + (x + dx) % SIDE) * 2 + core

    def behind(off):
        dz, dy, dx = off
        return ahead((SIDE - dz, SIDE - dy, SIDE - dx))

    def expert_ahead(off):
        dz, dy, _ = off
        return (((z + dz) % SIDE) * SIDE + (y + dy) % SIDE) // 2

    loads = [
        pltpu.make_async_copy(src, dst, small_sem.at[i])
        for i, (src, dst) in enumerate(((tokens_hbm, tokens), (gain_hbm, gain), (routes_hbm, routes), (mix_hbm, mix)))
    ]
    big = [
        pltpu.make_async_copy(src, dst, load_sem.at[i])
        for i, (src, dst) in enumerate(((gate_hbm, gate), (up_hbm, up), (down_hbm, down)))
    ]
    barrier = pltpu.get_barrier_semaphore()

    def greet(batch, i, carry):
        pl.semaphore_signal(barrier, inc=1, device_id=(ahead(offset_of(batch, i)),), device_id_type=MESH)
        return carry

    for copy in loads:
        copy.start()
    pl.semaphore_signal(barrier, inc=1, device_id=(partner,), device_id_type=MESH)
    for batch in range(BATCHES):
        lax.fori_loop(1 if batch == 0 else 0, PER, functools.partial(greet, batch), 0)
    for copy in big:
        copy.start()

    for copy in loads:
        copy.wait()
    values = tokens[...].astype(jnp.float32)
    scale = lax.rsqrt(jnp.mean(values * values, axis=-1, keepdims=True) + EPSILON)
    normed = values * scale * gain[...]
    slots = outgoing.shape[0] * 2
    ids = lax.broadcasted_iota(jnp.int32, (slots, 1), 0)
    expert, slot = ids // 2, ids % 2
    before = jnp.zeros((slots, 1), jnp.int32)
    picked = jnp.zeros((slots, width), jnp.float32)
    for t in range(count):
        named = (expert == routes[0, t]).astype(jnp.int32) + (expert == routes[1, t]).astype(jnp.int32)
        taken = (named == 1) & (before == slot)
        picked = jnp.where(taken, normed[t : t + 1, :], picked)
        before = before + named
    outgoing[...] = picked.astype(jnp.bfloat16).reshape(outgoing.shape)
    rows[0, 0, 0] = outgoing[expert_ahead((0, 0, 0))]

    pl.semaphore_wait(barrier, CHIPS)

    def dispatch(batch, i, carry):
        off = offset_of(batch, i)
        pltpu.make_async_remote_copy(
            src_ref=outgoing.at[expert_ahead(off)],
            dst_ref=rows.at[batch, 0, i],
            send_sem=disp_send,
            recv_sem=disp_recv.at[batch],
            device_id=(ahead(off),),
            device_id_type=MESH,
        ).start()
        return carry

    for batch in range(BATCHES):
        lax.fori_loop(1 if batch == 0 else 0, PER, functools.partial(dispatch, batch), 0)

    def give_back(batch, i, carry):
        off = offset_of(batch, i)
        pltpu.make_async_remote_copy(
            src_ref=summed.at[batch * PER + i],
            dst_ref=back.at[batch * PER + i],
            send_sem=back_send,
            recv_sem=back_recv,
            device_id=(behind(off),),
            device_id_type=MESH,
        ).start()
        return carry

    def to_partner(src, dst, send_sem, recv_sem):
        return pltpu.make_async_remote_copy(
            src_ref=src, dst_ref=dst, send_sem=send_sem, recv_sem=recv_sem, device_id=(partner,), device_id_type=MESH
        )

    nt = (((1,), (1,)), ((), ()))
    for batch in range(BATCHES):
        first = 1 if batch == 0 else 0
        block = rows.at[batch, 0, pl.ds(first, PER - first)]
        to_partner(block, block, disp_send, disp_recv.at[batch]).wait_recv()
        forward = to_partner(rows.at[batch, 0], rows.at[batch, 1], fwd_send.at[batch], fwd_recv.at[batch])
        forward.start()
        if batch == 0:
            for copy in big:
                copy.wait()
        forward.wait_recv()
        held = rows[batch].reshape(4 * PER, width)
        gated = lax.dot_general(held, gate[...], nt, preferred_element_type=jnp.float32)
        upper = lax.dot_general(held, up[...], nt, preferred_element_type=jnp.float32)
        hidden = (jax.nn.silu(gated) * upper).astype(jnp.bfloat16)
        theirs = jnp.dot(hidden[2 * PER :], down[...], preferred_element_type=jnp.float32)
        part_out[batch] = theirs.astype(jnp.bfloat16).reshape(PER, 2, width)
        reduce = to_partner(part_out.at[batch], part_in.at[batch], red_send.at[batch], red_recv.at[batch])
        reduce.start()
        own[...] = jnp.dot(hidden[: 2 * PER], down[...], preferred_element_type=jnp.float32)
        reduce.wait_recv()
        total = own[...] + part_in[batch].reshape(2 * PER, width).astype(jnp.float32)
        summed[pl.ds(batch * PER, PER)] = total.astype(jnp.bfloat16).reshape(PER, 2, width)
        if batch == 0:
            back[0] = summed[0]
        lax.fori_loop(first, PER, functools.partial(give_back, batch), 0)

    column = lax.broadcasted_iota(jnp.int32, (1, 2 * CHIPS), 1)
    dz, dy, _ = offset_of(0, column // 2)
    expert, slot = (((z + dz) % SIDE) * SIDE + (y + dy) % SIDE) // 2, column % 2
    before = jnp.zeros((1, 2 * CHIPS), jnp.int32)
    weights = []
    for t in range(count):
        first, second = expert == routes[0, t], expert == routes[1, t]
        named = first.astype(jnp.int32) + second.astype(jnp.int32)
        taken = (named == 1) & (before == slot)
        weights.append(jnp.where(taken, jnp.where(first, mix[0, t], mix[1, t]), 0.0))
        before = before + named
    high = [w.astype(jnp.bfloat16).astype(jnp.float32) for w in weights]
    low = [w - h for w, h in zip(weights, high)]
    lhs = jnp.concatenate(high + low, axis=0).astype(jnp.bfloat16)

    to_partner(back.at[pl.ds(1, CHIPS - 1)], back.at[pl.ds(1, CHIPS - 1)], back_send, back_recv).wait_recv()
    mixed = jnp.dot(lhs, back[...].reshape(2 * CHIPS, width), preferred_element_type=jnp.float32)
    out_ref[...] = (mixed[:count] + mixed[count:]).astype(out_ref.dtype)

    to_partner(back.at[pl.ds(1, CHIPS - 1)], back.at[pl.ds(1, CHIPS - 1)], disp_send, back_recv).wait_send()
    to_partner(back.at[pl.ds(1, CHIPS - 1)], back.at[pl.ds(1, CHIPS - 1)], back_send, back_recv).wait_send()
    for batch in range(BATCHES):
        to_partner(rows.at[batch, 0], rows.at[batch, 1], fwd_send.at[batch], fwd_recv.at[batch]).wait_send()
        to_partner(part_out.at[batch], part_in.at[batch], red_send.at[batch], red_recv.at[batch]).wait_send()


def on_device(tokens, norm_gain, routes, route_weight, gate_weight, up_weight, down_weight):
    count, width = tokens.shape
    hidden = gate_weight.shape[1]
    experts = 2 * CHIPS // GROUP
    bf16, f32 = jnp.bfloat16, jnp.float32
    return pl.pallas_call(
        kernel,
        out_shape=jax.ShapeDtypeStruct((count, width), bf16),
        in_specs=[pl.BlockSpec(memory_space=pltpu.HBM)] * 7,
        out_specs=pl.BlockSpec(memory_space=pltpu.VMEM),
        scratch_shapes=[
            pltpu.VMEM((count, width), bf16),
            pltpu.VMEM((1, width), f32),
            pltpu.SMEM((2, count), jnp.int32),
            pltpu.SMEM((2, count), f32),
            pltpu.VMEM((hidden, width), bf16),
            pltpu.VMEM((hidden, width), bf16),
            pltpu.VMEM((hidden, width), bf16),
            pltpu.VMEM((experts, 2, width), bf16),
            pltpu.VMEM((BATCHES, 2, PER, 2, width), bf16),
            pltpu.VMEM((BATCHES, PER, 2, width), bf16),
            pltpu.VMEM((BATCHES, PER, 2, width), bf16),
            pltpu.VMEM((2 * PER, width), f32),
            pltpu.VMEM((CHIPS, 2, width), bf16),
            pltpu.VMEM((CHIPS, 2, width), bf16),
            pltpu.SemaphoreType.DMA((3,)),
            pltpu.SemaphoreType.DMA((4,)),
            pltpu.SemaphoreType.DMA,
            pltpu.SemaphoreType.DMA((BATCHES,)),
            pltpu.SemaphoreType.DMA((BATCHES,)),
            pltpu.SemaphoreType.DMA((BATCHES,)),
            pltpu.SemaphoreType.DMA((BATCHES,)),
            pltpu.SemaphoreType.DMA((BATCHES,)),
            pltpu.SemaphoreType.DMA,
            pltpu.SemaphoreType.DMA,
        ],
        compiler_params=pltpu.CompilerParams(
            collective_id=0, has_side_effects=True, vmem_limit_bytes=67043328
        ),
        name="experts",
    )(tokens, norm_gain.reshape(1, width), routes.T, route_weight.T, gate_weight.T, up_weight.T, down_weight)


def solution(mesh):
    return jax.shard_map(
        on_device,
        mesh=mesh,
        in_specs=(
            P("ep", None),
            P(),
            P("ep", None),
            P("ep", None),
            P(None, "ep"),
            P(None, "ep"),
            P("ep", None),
        ),
        out_specs=P("ep", None),
        check_vma=False,
    )
```

time: 71.6 us -> 37.5 us (0.52)
  Pallas kernels: 0 us -> 35.7 us
  blocking collectives: 30.6 us -> 0 us
  waiting for transfers between devices: 19 us -> 0 us
  matrix products: 9.07 us -> 0 us
  local copies, waits for them, and re-layouts: 5.84 us -> 1.33 us
  starting transfers between devices: 4.42 us -> 0 us
  other arithmetic: 2.13 us -> 0 us
    pallas_call x0 -> x1, Pallas kernels: none -> 35.7 us  [on_device(): pl.pallas_call(kernel, out_shape=jax.ShapeDtypeStruct((count, width), bf1...]
    all_to_all x1 -> x0, blocking collectives: 30.6 us -> none  [on_device(): lax.all_to_all(outgoing, 'ep', split_axis=0, concat_axis=0, tiled=True)]
    all_to_all x1 -> x0, waiting for transfers between devices: 19 us -> none  [on_device(): lax.all_to_all(result.astype(jnp.bfloat16), 'ep', split_axis=0, concat_ax...]
    dot_general x6 -> x0, matrix products: 9.07 us -> none  [the longest x1 4.77 us: expert_rows(): return jnp.dot(hidden, down_part, preferred_element_type=jnp.float32)]
    all_to_all x1 -> x0, starting transfers between devices: 4.42 us -> none  [on_device(): lax.all_to_all(result.astype(jnp.bfloat16), 'ep', split_axis=0, concat_ax...]
    convert_element_type x1 -> x0, local copies, waits for them, and re-layouts: 2.56 us -> none  [on_device(): result.astype(jnp.bfloat16)]
    reduce_sum x3 -> x0, other arithmetic: 2 us -> none  [the longest x1 0.98 us: normalize(): jnp.mean(values * values, axis=-1, keepdims=True) + epsilon]
    reshape x3 -> x0, local copies, waits for them, and re-layouts: 1.64 us -> none  [the longest x1 1.46 us: on_device(): flat = received.reshape(devices * count, width)]
  transfers between devices with their start and end apart: 1 -> 0, of which waited for: 1 -> 0; matrix products, arithmetic and copies ran while one was open for 0% -> 0% of each run, Pallas kernels for 0% -> 0%
where the time goes in v1:
time: 37.5 us; the launch traced here: 37 us
  Pallas kernels  35.7 us (95%)
  local copies, waits for them, and re-layouts  1.33 us (4%)
    pallas_call x1, Pallas kernels, on_device(): pl.pallas_call(kernel, out_shape=jax.ShapeDtypeStruct((count, width), bf1...  35.7 us
    unnamed x1, local copies, waits for them, and re-layouts  1.33 us

profile of v1, /device:TPU:1, one launch (start us, length us, event | category | flops | bytes accessed | tf_op | source)
XLA Modules:
  0.0 37.0 jit_solution(15598513119747486559)
XLA Ops:
  0.0 35.7 %experts.1 = bf16[4,2048]{1,0:T(4,128)(2,1)} custom-call(bf16[4,2048]{1,0:T(4,128)(2,1)} %tokens_hbm.1, f32[1,2048]{1,0:T(1,128)} %bitcast.7, s32[2,4]{1,0:T(2,128)} %bitcast.8, f32[2,4]{1,0:T(2,128)} %bitcast.9, bf16[448,2048]{1,0:T(8,128)(2,1)} %bitcast.5, bf16[448,2048]{1,0:T(8,128)(2,1)} %bitcast.6, bf16[448,2048]{1,0:T(8,128)(2,1)} %down_hbm.1), custom_call_target="tpu_custom_call" | custom-call | tf_op jit(solution)/shard_map/experts/pallas_call | solution.py:183
  35.7 1.3 %copy.9 = bf16[4,2048]{1,0:T(4,128)(2,1)} copy(bf16[4,2048]{1,0:T(4,128)(2,1)} %experts.1) | data formatting | bytes 32768

commit v2 on v1

v2 whole, which is shorter than its diff:
```python
import functools

import jax
import jax.numpy as jnp
from jax import lax
from jax.experimental import pallas as pl
from jax.experimental.pallas import tpu as pltpu
from jax.sharding import PartitionSpec as P

MESH = pl.DeviceIdType.MESH
GROUP = 16
SIDE = 4
CHIPS = SIDE**3
EPSILON = 1e-06


def offset_of(k):
    return k // (SIDE * SIDE), (k // SIDE) % SIDE, k % SIDE


def kernel(
    tokens_hbm, gain_hbm, routes_hbm, mix_hbm, gate_hbm, up_hbm, down_hbm, out_ref,
    tokens, gain, routes, mix, gate, up, down, outgoing, rows, summed, back,
    load_sem, small_sem, share_send, share_recv, disp_send, disp_recv, back_send, back_recv, plane_sem, slice_sem,
):
    width = tokens.shape[1]
    count = tokens.shape[0]
    me = lax.axis_index("ep")
    core = me % 2
    chip = me // 2
    x, y, z = chip % SIDE, (chip // SIDE) % SIDE, chip // (SIDE * SIDE)
    partner = me + 1 - 2 * core

    def ahead(off):
        dz, dy, dx = off
        return ((((z + dz) % SIDE) * SIDE + (y + dy) % SIDE) * SIDE + (x + dx) % SIDE) * 2 + core

    def behind(off):
        dz, dy, dx = off
        return ahead((SIDE - dz, SIDE - dy, SIDE - dx))

    def expert_ahead(off):
        dz, dy, _ = off
        return (((z + dz) % SIDE) * SIDE + (y + dy) % SIDE) // 2

    loads = [
        pltpu.make_async_copy(src, dst, small_sem.at[i])
        for i, (src, dst) in enumerate(((tokens_hbm, tokens), (gain_hbm, gain), (routes_hbm, routes), (mix_hbm, mix)))
    ]
    big = [
        pltpu.make_async_copy(src, dst.at[0], load_sem.at[i])
        for i, (src, dst) in enumerate(((gate_hbm, gate), (up_hbm, up), (down_hbm, down)))
    ]
    barrier = pltpu.get_barrier_semaphore()

    for copy in loads:
        copy.start()
    pl.semaphore_signal(barrier, inc=1, device_id=(partner,), device_id_type=MESH)
    for step in range(1, SIDE):
        for off in ((0, 0, step), (0, step, 0), (step, 0, 0)):
            pl.semaphore_signal(barrier, inc=1, device_id=(ahead(off),), device_id_type=MESH)
    for copy in big:
        copy.start()

    for copy in loads:
        copy.wait()
    values = tokens[...].astype(jnp.float32)
    scale = lax.rsqrt(jnp.mean(values * values, axis=-1, keepdims=True) + EPSILON)
    normed = values * scale * gain[...]
    slots = outgoing.shape[0] * 2
    ids = lax.broadcasted_iota(jnp.int32, (slots, 1), 0)
    expert, slot = ids // 2, ids % 2
    before = jnp.zeros((slots, 1), jnp.int32)
    picked = jnp.zeros((slots, width), jnp.float32)
    for t in range(count):
        named = (expert == routes[0, t]).astype(jnp.int32) + (expert == routes[1, t]).astype(jnp.int32)
        taken = (named == 1) & (before == slot)
        picked = jnp.where(taken, normed[t : t + 1, :], picked)
        before = before + named
    outgoing[...] = picked.astype(jnp.bfloat16).reshape(outgoing.shape)
    rows[0] = outgoing[expert_ahead((0, 0, 0))]

    def to_partner(src, dst, send_sem, recv_sem):
        return pltpu.make_async_remote_copy(
            src_ref=src, dst_ref=dst, send_sem=send_sem, recv_sem=recv_sem, device_id=(partner,), device_id_type=MESH
        )

    shares = [
        to_partner(src, dst.at[1], share_send.at[i], share_recv.at[i])
        for i, (src, dst) in enumerate(((gate_hbm, gate), (up_hbm, up), (down_hbm, down)))
    ]

    def dispatch(k, carry):
        off = offset_of(k)
        pltpu.make_async_remote_copy(
            src_ref=outgoing.at[expert_ahead(off)],
            dst_ref=rows.at[k],
            send_sem=disp_send,
            recv_sem=disp_recv,
            device_id=(ahead(off),),
            device_id_type=MESH,
        ).start()
        return carry

    pl.semaphore_wait(barrier, 1 + 3 * (SIDE - 1))
    for step in range(1, SIDE):
        pl.semaphore_signal(plane_sem, inc=1, device_id=(ahead((0, step, 0)),), device_id_type=MESH)
    for step in range(1, SIDE):
        for k in (step, step * SIDE, step * SIDE * SIDE):
            dispatch(k, 0)
    for copy in shares:
        copy.start()
    pl.semaphore_wait(plane_sem, SIDE - 1)
    for step in range(1, SIDE):
        pl.semaphore_signal(slice_sem, inc=1, device_id=(ahead((step, 0, 0)),), device_id_type=MESH)
    for dy in range(1, SIDE):
        for dx in range(1, SIDE):
            dispatch(dy * SIDE + dx, 0)
    pl.semaphore_wait(slice_sem, SIDE - 1)
    for dz in (2, 1, 3):
        lax.fori_loop(dz * SIDE * SIDE + 1, (dz + 1) * SIDE * SIDE, dispatch, 0)

    def give_back(k, carry):
        pltpu.make_async_remote_copy(
            src_ref=summed.at[k],
            dst_ref=back.at[k],
            send_sem=back_send,
            recv_sem=back_recv,
            device_id=(behind(offset_of(k)),),
            device_id_type=MESH,
        ).start()
        return carry

    others = pl.ds(1, CHIPS - 1)
    nt = (((1,), (1,)), ((), ()))
    for copy in big:
        copy.wait()
    to_partner(rows.at[others], rows.at[others], disp_send, disp_recv).wait_recv()
    for copy in shares:
        copy.wait_recv()
    held = rows[...].reshape(2 * CHIPS, width)
    total = jnp.zeros((2 * CHIPS, width), jnp.float32)
    for part in range(2):
        gated = lax.dot_general(held, gate[part], nt, preferred_element_type=jnp.float32)
        upper = lax.dot_general(held, up[part], nt, preferred_element_type=jnp.float32)
        hidden = (jax.nn.silu(gated) * upper).astype(jnp.bfloat16)
        total = total + jnp.dot(hidden, down[part], preferred_element_type=jnp.float32)
    summed[...] = total.astype(jnp.bfloat16).reshape(CHIPS, 2, width)
    back[0] = summed[0]
    lax.fori_loop(1, CHIPS, give_back, 0)

    column = lax.broadcasted_iota(jnp.int32, (1, 2 * CHIPS), 1)
    dz, dy, _ = offset_of(column // 2)
    expert, slot = (((z + dz) % SIDE) * SIDE + (y + dy) % SIDE) // 2, column % 2
    before = jnp.zeros((1, 2 * CHIPS), jnp.int32)
    weights = []
    for t in range(count):
        first, second = expert == routes[0, t], expert == routes[1, t]
        named = first.astype(jnp.int32) + second.astype(jnp.int32)
        taken = (named == 1) & (before == slot)
        weights.append(jnp.where(taken, jnp.where(first, mix[0, t], mix[1, t]), 0.0))
        before = before + named
    high = [w.astype(jnp.bfloat16).astype(jnp.float32) for w in weights]
    low = [w - h for w, h in zip(weights, high)]
    lhs = jnp.concatenate(high + low, axis=0).astype(jnp.bfloat16)

    to_partner(back.at[others], back.at[others], back_send, back_recv).wait_recv()
    mixed = jnp.dot(lhs, back[...].reshape(2 * CHIPS, width), preferred_element_type=jnp.float32)
    out_ref[...] = (mixed[:count] + mixed[count:]).astype(out_ref.dtype)

    to_partner(rows.at[others], rows.at[others], disp_send, disp_recv).wait_send()
    to_partner(back.at[others], back.at[others], back_send, back_recv).wait_send()
    for copy in shares:
        copy.wait_send()


def on_device(tokens, norm_gain, routes, route_weight, gate_weight, up_weight, down_weight):
    count, width = tokens.shape
    hidden = gate_weight.shape[1]
    experts = 2 * CHIPS // GROUP
    bf16, f32 = jnp.bfloat16, jnp.float32
    return pl.pallas_call(
        kernel,
        out_shape=jax.ShapeDtypeStruct((count, width), bf16),
        in_specs=[pl.BlockSpec(memory_space=pltpu.HBM)] * 7,
        out_specs=pl.BlockSpec(memory_space=pltpu.VMEM),
        scratch_shapes=[
            pltpu.VMEM((count, width), bf16),
            pltpu.VMEM((1, width), f32),
            pltpu.SMEM((2, count), jnp.int32),
            pltpu.SMEM((2, count), f32),
            pltpu.VMEM((2, hidden, width), bf16),
            pltpu.VMEM((2, hidden, width), bf16),
            pltpu.VMEM((2, hidden, width), bf16),
            pltpu.VMEM((experts, 2, width), bf16),
            pltpu.VMEM((CHIPS, 2, width), bf16),
            pltpu.VMEM((CHIPS, 2, width), bf16),
            pltpu.VMEM((CHIPS, 2, width), bf16),
            pltpu.SemaphoreType.DMA((3,)),
            pltpu.SemaphoreType.DMA((4,)),
            pltpu.SemaphoreType.DMA((3,)),
            pltpu.SemaphoreType.DMA((3,)),
            pltpu.SemaphoreType.DMA,
            pltpu.SemaphoreType.DMA,
            pltpu.SemaphoreType.DMA,
            pltpu.SemaphoreType.DMA,
            pltpu.SemaphoreType.REGULAR,
            pltpu.SemaphoreType.REGULAR,
        ],
        compiler_params=pltpu.CompilerParams(
            collective_id=0, has_side_effects=True, vmem_limit_bytes=67043328
        ),
        name="experts",
    )(tokens, norm_gain.reshape(1, width), routes.T, route_weight.T, gate_weight.T, up_weight.T, down_weight)


def solution(mesh):
    return jax.shard_map(
        on_device,
        mesh=mesh,
        in_specs=(
            P("ep", None),
            P(),
            P("ep", None),
            P("ep", None),
            P(None, "ep"),
            P(None, "ep"),
            P("ep", None),
        ),
        out_specs=P("ep", None),
        check_vma=False,
    )
```

time: 37.5 us -> 32.9 us (0.88)
  the two profiles are of different devices: /device:TPU:1 before, /device:TPU:0 now
where the time goes in v2:
time: 32.9 us; the launch traced here: 32.7 us
  Pallas kernels  31.3 us (95%)
  local copies, waits for them, and re-layouts  1.33 us (4%)
    pallas_call x1, Pallas kernels, on_device(): pl.pallas_call(kernel, out_shape=jax.ShapeDtypeStruct((count, width), bf1...  31.3 us
    unnamed x1, local copies, waits for them, and re-layouts  1.33 us

profile of v2, /device:TPU:0, one launch (start us, length us, event | category | flops | bytes accessed | tf_op | source)
XLA Modules:
  0.0 32.7 jit_solution(9474365271876496066)
XLA Ops:
  0.0 31.3 %experts.1 = bf16[4,2048]{1,0:T(4,128)(2,1)} custom-call(bf16[4,2048]{1,0:T(4,128)(2,1)} %tokens_hbm.1, f32[1,2048]{1,0:T(1,128)} %bitcast.7, s32[2,4]{1,0:T(2,128)} %bitcast.8, f32[2,4]{1,0:T(2,128)} %bitcast.9, bf16[448,2048]{1,0:T(8,128)(2,1)} %bitcast.5, bf16[448,2048]{1,0:T(8,128)(2,1)} %bitcast.6, bf16[448,2048]{1,0:T(8,128)(2,1)} %down_hbm.1), custom_call_target="tpu_custom_call" | custom-call | tf_op jit(solution)/shard_map/experts/pallas_call | solution.py:182
  31.4 1.3 %copy.9 = bf16[4,2048]{1,0:T(4,128)(2,1)} copy(bf16[4,2048]{1,0:T(4,128)(2,1)} %experts.1) | data formatting | bytes 32768

commit v3 on v2

v3 whole, which is shorter than its diff:
```python
import functools

import jax
import jax.numpy as jnp
from jax import lax
from jax.experimental import pallas as pl
from jax.experimental.pallas import tpu as pltpu
from jax.sharding import PartitionSpec as P

MESH = pl.DeviceIdType.MESH
GROUP = 16
SIDE = 4
CHIPS = SIDE**3
EPSILON = 1e-06
BATCHES = 2
PER = CHIPS // BATCHES
SHARE = GROUP // 2


def kernel(
    tokens_hbm, gain_hbm, routes_hbm, mix_hbm, gate_hbm, up_hbm, down_hbm, out_ref,
    tokens, gain, routes, mix, gate, up, down, outgoing, rows, summed, back,
    gate_t, up_t,
    load_sem, small_sem, share_send, share_recv, disp_send, disp_recv, back_send, back_recv, plane_sem, slice_sem,
):
    width = tokens.shape[1]
    count = tokens.shape[0]
    me = lax.axis_index("ep")
    core = me % 2
    chip = me // 2
    x, y, z = chip % SIDE, (chip // SIDE) % SIDE, chip // (SIDE * SIDE)
    partner = me + 1 - 2 * core

    def chip_ahead(dz, dy, dx):
        return (((z + dz) % SIDE) * SIDE + (y + dy) % SIDE) * SIDE + (x + dx) % SIDE

    def device(other):
        return (2 * other + core,)

    loads = [
        pltpu.make_async_copy(src, dst, small_sem.at[i])
        for i, (src, dst) in enumerate(((tokens_hbm, tokens), (gain_hbm, gain), (routes_hbm, routes), (mix_hbm, mix)))
    ]
    big = [
        pltpu.make_async_copy(src, dst.at[0], load_sem.at[i])
        for i, (src, dst) in enumerate(((gate_hbm, gate), (up_hbm, up), (down_hbm, down)))
    ]
    barrier = pltpu.get_barrier_semaphore()

    for copy in loads:
        copy.start()
    pl.semaphore_signal(barrier, inc=1, device_id=(partner,), device_id_type=MESH)
    for step in range(1, SIDE):
        for off in ((0, 0, step), (0, step, 0), (step, 0, 0)):
            pl.semaphore_signal(barrier, inc=1, device_id=device(chip_ahead(*off)), device_id_type=MESH)
    for copy in big:
        copy.start()

    for copy in loads:
        copy.wait()
    values = tokens[...].astype(jnp.float32)
    scale = lax.rsqrt(jnp.mean(values * values, axis=-1, keepdims=True) + EPSILON)
    normed = values * scale * gain[...]
    slots = outgoing.shape[0] * 2
    ids = lax.broadcasted_iota(jnp.int32, (slots, 1), 0)
    expert, slot = ids // 2, ids % 2
    before = jnp.zeros((slots, 1), jnp.int32)
    picked = jnp.zeros((slots, width), jnp.float32)
    for t in range(count):
        named = (expert == routes[0, t]).astype(jnp.int32) + (expert == routes[1, t]).astype(jnp.int32)
        taken = (named == 1) & (before == slot)
        picked = jnp.where(taken, normed[t : t + 1, :], picked)
        before = before + named
    outgoing[...] = picked.astype(jnp.bfloat16).reshape(outgoing.shape)
    rows[chip] = outgoing[chip // SHARE]

    def to_partner(src, dst, send_sem, recv_sem):
        return pltpu.make_async_remote_copy(
            src_ref=src, dst_ref=dst, send_sem=send_sem, recv_sem=recv_sem, device_id=(partner,), device_id_type=MESH
        )

    shares = [
        to_partner(src, dst.at[1], share_send.at[i], share_recv.at[i])
        for i, (src, dst) in enumerate(((gate_hbm, gate), (up_hbm, up), (down_hbm, down)))
    ]

    def dispatch(dz, dy, dx):
        other = chip_ahead(dz, dy, dx)
        pltpu.make_async_remote_copy(
            src_ref=outgoing.at[other // SHARE],
            dst_ref=rows.at[chip],
            send_sem=disp_send,
            recv_sem=disp_recv.at[chip // PER],
            device_id=device(other),
            device_id_type=MESH,
        ).start()

    def dispatch_plane(dz, j, carry):
        dispatch(dz, j // SIDE, j % SIDE)
        return carry

    pl.semaphore_wait(barrier, 1 + 3 * (SIDE - 1))
    for step in range(1, SIDE):
        pl.semaphore_signal(plane_sem, inc=1, device_id=device(chip_ahead(0, step, 0)), device_id_type=MESH)
    for step in range(1, SIDE):
        dispatch(0, 0, step)
        dispatch(0, step, 0)
        dispatch(step, 0, 0)
    for copy in shares:
        copy.start()
    pl.semaphore_wait(plane_sem, SIDE - 1)
    for step in range(1, SIDE):
        pl.semaphore_signal(slice_sem, inc=1, device_id=device(chip_ahead(step, 0, 0)), device_id_type=MESH)
    for dy in range(1, SIDE):
        for dx in range(1, SIDE):
            dispatch(0, dy, dx)
    pl.semaphore_wait(slice_sem, SIDE - 1)
    for dz in (2, 1, 3):
        lax.fori_loop(1, SIDE * SIDE, functools.partial(dispatch_plane, dz), 0)

    def give_back(batch, i, carry):
        other = batch * PER + (chip + i) % PER
        pltpu.make_async_remote_copy(
            src_ref=summed.at[other],
            dst_ref=back.at[chip],
            send_sem=back_send,
            recv_sem=back_recv,
            device_id=device(other),
            device_id_type=MESH,
        ).start()
        return carry

    def transpose(part):
        gate_t[part] = gate[part].T
        up_t[part] = up[part].T

    for copy in big:
        copy.wait()
    transpose(0)
    shares[0].wait_recv()
    shares[1].wait_recv()
    transpose(1)
    shares[2].wait_recv()
    for batch in range(BATCHES):
        mine = chip // PER == batch
        for other, held in ((mine, PER - 1), (jnp.logical_not(mine), PER)):
            @pl.when(other)
            def _():
                block = rows.at[pl.ds(0, held)]
                to_partner(block, block, disp_send, disp_recv.at[batch]).wait_recv()

        lhs = rows[pl.ds(batch * PER, PER)].reshape(2 * PER, width)
        total = jnp.zeros((2 * PER, width), jnp.float32)
        for part in range(2):
            gated = jnp.dot(lhs, gate_t[part], preferred_element_type=jnp.float32)
            upper = jnp.dot(lhs, up_t[part], preferred_element_type=jnp.float32)
            hidden = (jax.nn.silu(gated) * upper).astype(jnp.bfloat16)
            total = total + jnp.dot(hidden, down[part], preferred_element_type=jnp.float32)
        summed[pl.ds(batch * PER, PER)] = total.astype(jnp.bfloat16).reshape(PER, 2, width)

        @pl.when(mine)
        def _():
            back[chip] = summed[chip]

        lax.fori_loop(mine.astype(jnp.int32), PER, functools.partial(give_back, batch), 0)

    column = lax.broadcasted_iota(jnp.int32, (1, 2 * CHIPS), 1)
    expert, slot = column // (2 * SHARE), column % 2
    before = jnp.zeros((1, 2 * CHIPS), jnp.int32)
    weights = []
    for t in range(count):
        first, second = expert == routes[0, t], expert == routes[1, t]
        named = first.astype(jnp.int32) + second.astype(jnp.int32)
        taken = (named == 1) & (before == slot)
        weights.append(jnp.where(taken, jnp.where(first, mix[0, t], mix[1, t]), 0.0))
        before = before + named
    high = [w.astype(jnp.bfloat16).astype(jnp.float32) for w in weights]
    low = [w - h for w, h in zip(weights, high)]
    lhs = jnp.concatenate(high + low, axis=0).astype(jnp.bfloat16)

    others = pl.ds(0, CHIPS - 1)
    to_partner(back.at[others], back.at[others], back_send, back_recv).wait_recv()
    mixed = jnp.dot(lhs, back[...].reshape(2 * CHIPS, width), preferred_element_type=jnp.float32)
    out_ref[...] = (mixed[:count] + mixed[count:]).astype(out_ref.dtype)

    to_partner(rows.at[others], rows.at[others], disp_send, disp_recv.at[0]).wait_send()
    to_partner(back.at[others], back.at[others], back_send, back_recv).wait_send()
    for copy in shares:
        copy.wait_send()


def on_device(tokens, norm_gain, routes, route_weight, gate_weight, up_weight, down_weight):
    count, width = tokens.shape
    hidden = gate_weight.shape[1]
    experts = 2 * CHIPS // GROUP
    bf16, f32 = jnp.bfloat16, jnp.float32
    return pl.pallas_call(
        kernel,
        out_shape=pltpu.VMEM((count, width), bf16),
        in_specs=[pl.BlockSpec(memory_space=pltpu.HBM)] * 7,
        out_specs=pl.BlockSpec(memory_space=pltpu.VMEM),
        scratch_shapes=[
            pltpu.VMEM((count, width), bf16),
            pltpu.VMEM((1, width), f32),
            pltpu.SMEM((2, count), jnp.int32),
            pltpu.SMEM((2, count), f32),
            pltpu.VMEM((2, hidden, width), bf16),
            pltpu.VMEM((2, hidden, width), bf16),
            pltpu.VMEM((2, hidden, width), bf16),
            pltpu.VMEM((experts, 2, width), bf16),
            pltpu.VMEM((CHIPS, 2, width), bf16),
            pltpu.VMEM((CHIPS, 2, width), bf16),
            pltpu.VMEM((CHIPS, 2, width), bf16),
            pltpu.VMEM((2, width, hidden), bf16),
            pltpu.VMEM((2, width, hidden), bf16),
            pltpu.SemaphoreType.DMA((3,)),
            pltpu.SemaphoreType.DMA((4,)),
            pltpu.SemaphoreType.DMA((3,)),
            pltpu.SemaphoreType.DMA((3,)),
            pltpu.SemaphoreType.DMA,
            pltpu.SemaphoreType.DMA((BATCHES,)),
            pltpu.SemaphoreType.DMA,
            pltpu.SemaphoreType.DMA,
            pltpu.SemaphoreType.REGULAR,
            pltpu.SemaphoreType.REGULAR,
        ],
        compiler_params=pltpu.CompilerParams(
            collective_id=0, has_side_effects=True, vmem_limit_bytes=67043328 - 2**17
        ),
        name="experts",
    )(tokens, norm_gain.reshape(1, width), routes.T, route_weight.T, gate_weight.T, up_weight.T, down_weight)


def solution(mesh):
    return jax.shard_map(
        on_device,
        mesh=mesh,
        in_specs=(
            P("ep", None),
            P(),
            P("ep", None),
            P("ep", None),
            P(None, "ep"),
            P(None, "ep"),
            P("ep", None),
        ),
        out_specs=P("ep", None),
        check_vma=False,
    )
```

time: 32.9 us -> 28.9 us (0.88)
  the two profiles are of different devices: /device:TPU:0 before, /device:TPU:96 now
where the time goes in v3:
time: 28.9 us; the launch traced here: 28.7 us
  Pallas kernels  28.1 us (97%)
  local copies, waits for them, and re-layouts  0.61 us (2%)
    pallas_call x1, Pallas kernels, on_device(): pl.pallas_call(kernel, out_shape=pltpu.VMEM((count, width), bf16), in_spe...  28.1 us
    unnamed x1, local copies, waits for them, and re-layouts  0.61 us

profile of v3, /device:TPU:96, one launch (start us, length us, event | category | flops | bytes accessed | tf_op | source)
XLA Modules:
  0.0 28.7 jit_solution(5484895642050713666)
XLA Ops:
  0.0 28.1 %experts.1 = bf16[4,2048]{1,0:T(4,128)(2,1)S(1)} custom-call(bf16[4,2048]{1,0:T(4,128)(2,1)} %tokens_hbm.1, f32[1,2048]{1,0:T(1,128)} %bitcast.7, s32[2,4]{1,0:T(2,128)} %bitcast.8, f32[2,4]{1,0:T(2,128)} %bitcast.9, bf16[448,2048]{1,0:T(8,128)(2,1)} %bitcast.5, bf16[448,2048]{1,0:T(8,128)(2,1)} %bitcast.6, bf16[448,2048]{1,0:T(8,128)(2,1)} %down_hbm.1), custom_call_target="tpu_custom_call" | custom-call | tf_op jit(solution)/shard_map/experts/pallas_call | solution.py:197
  28.1 0.6 %copy.9 = bf16[4,2048]{1,0:T(4,128)(2,1)} copy(bf16[4,2048]{1,0:T(4,128)(2,1)S(1)} %experts.1) | data formatting | bytes 32768
